TPU v7x, 256 devices: a whole 4x4x8 slice. The times are simulated.
256 devices in a mesh: sp: 64 (over z, x, core), tp: 4 (over y).
Axes of the slice: x: 4, y: 4, z: 8, core: 2. Of those that a mesh axis runs over, the one named last changes fastest.
Arguments:
- residual: bfloat16 [16384, 2048], P(('sp', 'tp')), may hold values from -6 to 6
- query_wide: bfloat16 [16384, 512], P('sp', 'tp'), may hold values from -8 to 8
- key_wide: bfloat16 [16384, 512], P('sp', 'tp'), may hold values from -8 to 8
- value_wide: bfloat16 [16384, 512], P('sp', 'tp'), may hold values from -6 to 6
- query_narrow: bfloat16 [16384, 512], P('sp', 'tp'), may hold values from -8 to 8
- key_narrow: bfloat16 [16384, 512], P('sp', 'tp'), may hold values from -8 to 8
- value_narrow: bfloat16 [16384, 512], P('sp', 'tp'), may hold values from -6 to 6
- gate_wide: float32 [16384, 4], P('sp', 'tp'), may hold values from -2 to 20
- gate_narrow: float32 [16384, 8], P('sp', 'tp'), may hold values from -2 to 20
- out_wide: bfloat16 [512, 2048], replicated, may hold values from -0.1875 to 0.1875
- out_narrow: bfloat16 [512, 2048], replicated, may hold values from -0.1875 to 0.1875
- norm_gain: float32 [2048], replicated, may hold values from 0.1 to 1.9
- routing: int32 [16384, 2], P(('sp', 'tp')), may hold values from 0 to 63, as said below
- route_weight: float32 [16384, 2], P(('sp', 'tp')), may hold values from 0.3 to 1.5
- gate_weight: bfloat16 [64, 2048, 1024], P('sp', None, 'tp'), may hold values from -0.125 to 0.125
- up_weight: bfloat16 [64, 2048, 1024], P('sp', None, 'tp'), may hold values from -0.125 to 0.125
- down_weight: bfloat16 [64, 1024, 2048], P('sp', 'tp'), may hold values from -0.1875 to 0.1875
Outputs:
- result: bfloat16 [16384, 2048], P(('sp', 'tp'))
Inputs may be any that keep to these rules, and one draw needn't show every extreme that they name: `routing`: each row names 2 different experts of one group (experts g * 16 to g * 16 + 15). In each aligned block of 64 rows (the rows of one device) no expert is named by more than 4 rows; one group, the same for all blocks, has each of its experts named by exactly 4 rows of every block.
All inputs are finite; a program needn't handle non-finite values.
Results may differ from a plain program's by a relative error of at most 0.017.
Values may be sent and summed in bfloat16 or wider, within the bound.
A program may use at most 128 MiB of HBM per device.

v0:
```python
import math
import jax
import jax.numpy as jnp
from jax import lax
from jax.sharding import PartitionSpec as P

HW = 128
HN = 64
GROUPS = 4
epsilon = 1e-06


def sent_together(arrays, axis, dim, along):
    both = jnp.concatenate(arrays, axis=along)
    whole, at, outs = (lax.all_gather(both, axis, axis=dim, tiled=True), 0, [])
    for a in arrays:
        outs.append(lax.slice_in_dim(whole, at, at + a.shape[along], axis=along))
        at += a.shape[along]
    return tuple(outs)


def globalize(pieces, shard_rows):
    shards = pieces.shape[0] // shard_rows
    grid = pieces.reshape(shards, shard_rows, pieces.shape[1])
    endings = grid[:, -1, :]
    offsets = jnp.cumsum(endings, axis=0) - endings
    return (grid + offsets[:, None, :]).reshape(pieces.shape)


def head_block(
    state, queries, query_decay, keys, values, key_decay, first_key, first_query, head_width
):
    highest_old, weight_sum, weighted = state
    query_rows = queries.shape[0]
    head_count = query_decay.shape[1]
    key_rows = keys.shape[0]
    grid_query = queries.reshape(query_rows, head_count, head_width)
    grid_key = keys.reshape(key_rows, head_count, head_width)
    grid_value = values.reshape(key_rows, head_count, head_width)
    scores = jnp.einsum("thd,phd->htp", grid_query, grid_key, preferred_element_type=jnp.float32)
    scores = scores * head_width ** (-0.5) + query_decay.T[:, :, None] - key_decay.T[:, None, :]
    query_place = first_query + jnp.arange(query_rows, dtype=jnp.int32)
    key_place = first_key + jnp.arange(key_rows, dtype=jnp.int32)
    scores = jnp.where(key_place[None, None, :] <= query_place[None, :, None], scores, -jnp.inf)
    highest = jnp.maximum(highest_old, jnp.max(scores, axis=2))
    weights = jnp.exp(scores - highest[:, :, None])
    shrink = jnp.exp(highest_old - highest)
    weight_sum = weight_sum * shrink + jnp.sum(weights, axis=2)
    product = jnp.einsum(
        "htp,phd->htd", weights.astype(jnp.bfloat16), grid_value, preferred_element_type=jnp.float32
    )
    weighted = weighted * shrink[:, :, None] + product
    return (highest, weight_sum, weighted)


def fresh_state(head_count, shard_rows, head_width):
    return (
        jnp.full((head_count, shard_rows), -1e30, jnp.float32),
        jnp.zeros((head_count, shard_rows), jnp.float32),
        jnp.zeros((head_count, shard_rows, head_width), jnp.float32),
    )


def finish(state, shard_rows):
    highest, weight_sum, weighted = state
    mixed_heads = weighted / weight_sum[:, :, None]
    joined = jnp.transpose(mixed_heads, (1, 0, 2))
    return joined.reshape(shard_rows, weighted.shape[0] * weighted.shape[2]).astype(jnp.bfloat16)


def body(
    residual,
    query_wide,
    key_wide,
    value_wide,
    query_narrow,
    key_narrow,
    value_narrow,
    gate_wide,
    gate_narrow,
    out_wide,
    out_narrow,
    norm_gain,
    routing,
    route_weight,
    gate_weight,
    up_weight,
    down_weight,
):
    shard_rows = query_wide.shape[0]
    half_rows = shard_rows // 2
    sp_place = lax.axis_index("sp")
    first_query = sp_place * shard_rows
    running_wide = jnp.cumsum(jax.nn.log_sigmoid(gate_wide), axis=0)
    running_narrow = jnp.cumsum(jax.nn.log_sigmoid(gate_narrow), axis=0)
    pieces_wide, pieces_narrow = sent_together((running_wide, running_narrow), "sp", 0, 1)
    every_wide = globalize(pieces_wide, shard_rows)
    every_narrow = globalize(pieces_narrow, shard_rows)
    late_first = first_query + half_rows
    halves = []
    for place, part_wide, part_narrow in (
        (first_query, query_wide[:half_rows], query_narrow[:half_rows]),
        (late_first, query_wide[half_rows:], query_narrow[half_rows:]),
    ):
        halves.append(
            (
                place,
                part_wide,
                part_narrow,
                lax.dynamic_slice_in_dim(every_wide, place, half_rows, 0),
                lax.dynamic_slice_in_dim(every_narrow, place, half_rows, 0),
            )
        )

    def half_state():
        return (
            fresh_state(gate_wide.shape[1], half_rows, HW),
            fresh_state(gate_narrow.shape[1], half_rows, HN),
        )

    state = (half_state(), half_state())
    keys_wide, values_wide, keys_narrow, values_narrow = sent_together(
        (key_wide, value_wide, key_narrow, value_narrow), "sp", 0, 1
    )
    span_rows = keys_wide.shape[0]
    block_size = math.gcd(span_rows, 2048)

    def visit(carried, position):
        inside = position * block_size

        def take_block(source):
            return lax.dynamic_slice_in_dim(source, inside, block_size, 0)

        def take_decay(source):
            return lax.dynamic_slice_in_dim(source, inside, block_size, 0)

        block_kw = take_block(keys_wide)
        block_vw = take_block(values_wide)
        block_kn = take_block(keys_narrow)
        block_vn = take_block(values_narrow)
        block_dw = take_decay(every_wide)
        block_dn = take_decay(every_narrow)

        def one_half(current, half):
            place, part_wide, part_narrow, query_decay_wide, query_decay_narrow = half

            def work(inner):
                first = head_block(
                    inner[0],
                    part_wide,
                    query_decay_wide,
                    block_kw,
                    block_vw,
                    block_dw,
                    inside,
                    place,
                    HW,
                )
                second = head_block(
                    inner[1],
                    part_narrow,
                    query_decay_narrow,
                    block_kn,
                    block_vn,
                    block_dn,
                    inside,
                    place,
                    HN,
                )
                return (first, second)

            def skip(inner):
                return inner

            return lax.cond(inside <= place + half_rows - 1, work, skip, current)

        updated = (one_half(carried[0], halves[0]), one_half(carried[1], halves[1]))
        return (updated, None)

    state, _ = lax.scan(visit, state, jnp.arange(span_rows // block_size, dtype=jnp.int32))
    att_wide = jnp.concatenate(
        [finish(state[0][0], half_rows), finish(state[1][0], half_rows)], axis=0
    )
    att_narrow = jnp.concatenate(
        [finish(state[0][1], half_rows), finish(state[1][1], half_rows)], axis=0
    )
    own_rows = residual.shape[0]
    heads_wide, heads_narrow = (
        lax.all_to_all(att_wide, "tp", split_axis=0, concat_axis=1, tiled=True),
        lax.all_to_all(att_narrow, "tp", split_axis=0, concat_axis=1, tiled=True),
    )
    mixed = jnp.dot(heads_wide, out_wide, preferred_element_type=jnp.float32)
    mixed = mixed + jnp.dot(heads_narrow, out_narrow, preferred_element_type=jnp.float32)
    middle = (residual.astype(jnp.float32) + mixed).astype(jnp.bfloat16)
    middle_wide = middle.astype(jnp.float32)
    spread = jnp.mean(middle_wide * middle_wide, axis=1, keepdims=True)
    normed = (middle_wide * lax.rsqrt(spread + epsilon) * norm_gain).astype(jnp.bfloat16)
    features = normed.shape[1]
    chosen_count = routing.shape[1]
    expert_count = gate_weight.shape[0] * lax.axis_size("sp")
    capacity = own_rows * GROUPS // expert_count
    flat_routes = routing.reshape(-1)
    matches = (flat_routes[:, None] == jnp.arange(expert_count, dtype=jnp.int32)[None, :]).astype(
        jnp.int32
    )
    ranking = jnp.sum((jnp.cumsum(matches, axis=0) - matches) * matches, axis=1)
    placing = flat_routes * capacity + ranking
    picker = (
        placing[None, :] == jnp.arange(expert_count * capacity, dtype=jnp.int32)[:, None]
    ).astype(jnp.bfloat16)
    picker = jnp.sum(picker.reshape(expert_count * capacity, own_rows, chosen_count), axis=2)
    outgoing = jnp.dot(picker, normed, preferred_element_type=jnp.float32).astype(jnp.bfloat16)
    outgoing = outgoing.reshape(expert_count, capacity, features)
    arrived = lax.all_to_all(outgoing, "sp", split_axis=0, concat_axis=0, tiled=True)
    pooled = lax.all_gather(arrived.reshape(-1, features), "tp", axis=0, tiled=True)
    gate_value = jnp.dot(pooled, gate_weight[0], preferred_element_type=jnp.float32)
    up_value = jnp.dot(pooled, up_weight[0], preferred_element_type=jnp.float32)
    hidden = (jax.nn.silu(gate_value) * up_value).astype(jnp.bfloat16)
    answers = lax.psum_scatter(
        jnp.dot(hidden, down_weight[0], preferred_element_type=jnp.float32).astype(jnp.bfloat16),
        "tp",
        scatter_dimension=0,
        tiled=True,
    )
    returned = lax.all_to_all(
        answers.reshape(expert_count, capacity, features),
        "sp",
        split_axis=0,
        concat_axis=0,
        tiled=True,
    )
    picked = jnp.take(returned.reshape(expert_count * capacity, features), placing, axis=0)
    picked = picked.reshape(own_rows, chosen_count, features).astype(jnp.float32)
    combined = jnp.sum(route_weight[:, :, None] * picked, axis=1)
    return (middle_wide + combined).astype(jnp.bfloat16)


def solution(mesh):
    placed = (
        P(("sp", "tp"), None),
        P("sp", "tp"),
        P("sp", "tp"),
        P("sp", "tp"),
        P("sp", "tp"),
        P("sp", "tp"),
        P("sp", "tp"),
        P("sp", "tp"),
        P("sp", "tp"),
        P(),
        P(),
        P(),
        P(("sp", "tp"), None),
        P(("sp", "tp"), None),
        P("sp", None, "tp"),
        P("sp", None, "tp"),
        P("sp", "tp", None),
    )
    return jax.shard_map(
        body, mesh=mesh, in_specs=placed, out_specs=P(("sp", "tp"), None), check_vma=False
    )
```

profile of v0, /device:TPU:1, one launch (start us, length us, event | category | flops | bytes accessed | tf_op | source)
XLA Modules:
  0.0 530.6 jit_solution(731115562800236567)
XLA Ops:
  18.2 48.7 %all_gather.10 = f32[16384,3]{0,1:T(4,128)S(1)} all-gather(f32[256,3]{0,1:T(4,128)S(1)} %pad_maximum_fusion.3), channel_id=1, replica_groups=mesh['sp'=64,'tp'=4] {'sp'}, dimensions={0}, use_global_device_ids=true | all-gather | bytes 199680 | tf_op jit(solution)/shard_map/all_gather | solution.py:15
  67.1 4.9 copy.106
  72.0 1.2 reduce-window_subtract_fusion
  73.7 9.2 %reshape.388 = f32[64,256,1]{2,1,0:T(8,128)} reshape(f32[16384]{0:T(1024)S(1)} %slice_reduce_fusion) | data formatting | bytes 131072 | tf_op jit(solution)/shard_map/reshape | solution.py:24
  82.9 1.7 fusion.75
  85.5 1.2 constant_dynamic-slice_fusion.7
  89.4 32.0 %all-gather.3.cloned.1.call-done = bf16[16384,512]{0,1:T(8,128)(2,1)} async-done(((bf16[256,512]{0,1:T(8,128)(2,1)}), bf16[16384,512]{0,1:T(8,128)(2,1)}) %all-gather.3.cloned.1.call-update) | async-done | bytes 16777232 | tf_op jit(solution)/shard_map/all_gather | solution.py:15
  121.4 12.1 %fusion.72 = (bf16[16384,128]{0,1:T(8,128)(2,1)}, bf16[16384,128]{0,1:T(8,128)(2,1)}, bf16[16384,128]{0,1:T(8,128)(2,1)}, bf16[16384,128]{0,1:T(8,128)(2,1)}) fusion(bf16[16384,512]{0,1:T(8,128)(2,1)} %all-gather.3.cloned.1.call-done), kind=kLoop, calls=%fused_computation.146 | loop fusion | bytes 33554432 | tf_op jit(solution)/shard_map/slice | solution.py:17
  138.6 89.0 %while.35 = (s32[]{:T(128)}, f32[1,128]{1,0:T(1,128)}, f32[1,128]{1,0:T(1,128)}, f32[1,128,128]{2,1,0:T(8,128)S(1)}, f32[2,128]{1,0:T(2,128)}, /*index=5*/f32[2,...) while((s32[]{:T(128)}, f32[1,128]{1,0:T(1,128)}, ...), condition=%wide.region_19.20_spmd, body=%wide.region_6.19_spmd.sunk | while | flops 552212480 | bytes 35769752 | solution.py:180
  138.6 1.2 dynamic_slice.78
  140.5 1.3 constant_dynamic-slice_fusion.15
  141.8 2.1 constant_dynamic-slice_fusion.16
  143.8 2.1 constant_dynamic-slice_fusion.14
  146.9 1.3 copy.144
  148.2 5.7 %conditional.4 = ((f32[1,128]{1,0:T(1,128)}, f32[1,128]{1,0:T(1,128)}, f32[1,128,128]{2,1,0:T(8,128)S(1)}, f32[2,128]{1,0:T(2,128)}, f32[2,128]{1,0:T(2,128)}, /*index=5*/f32[2,128,64]{1,2,0:T(8,128)S(1)})) conditional(s32[]{:T(128)} %convert_element_type.151, (f32[1,128]{1,0:T(1,128)}, f32[1,128]{1,0:T(1,128)}, f32[1,128,128]{2,1,0:T(8,128)S(1)}, ...), branch_computations={%region_7.7_spmd, %region_8.12_spmd} | conditional | flops 276106240 | bytes 14714172 | solution.py:175
  148.6 1.5 fusion.68
  153.9 5.6 %conditional.5 = ((f32[1,128]{1,0:T(1,128)}, f32[1,128]{1,0:T(1,128)}, f32[1,128,128]{2,1,0:T(8,128)S(1)}, f32[2,128]{1,0:T(2,128)}, f32[2,128]{1,0:T(2,128)}, /*index=5*/f32[2,128,64]{1,2,0:T(8,128)S(1)})) conditional(s32[]{:T(128)} %convert_element_type.152, (f32[1,128]{1,0:T(1,128)}, f32[1,128]{1,0:T(1,128)}, f32[1,128,128]{2,1,0:T(8,128)S(1)}, ...), branch_computations={%region_13.13_spmd, %region_14.18_spmd} | conditional | flops 276106240 | bytes 14714172 | solution.py:175
  154.2 1.5 fusion.70
  161.4 1.3 constant_dynamic-slice_fusion.15
  162.7 2.1 constant_dynamic-slice_fusion.16
  164.7 2.1 constant_dynamic-slice_fusion.14
  167.8 1.3 copy.144
  171.1 1.3 constant_dynamic-slice_fusion.15
  172.4 2.1 constant_dynamic-slice_fusion.16
  174.5 2.1 constant_dynamic-slice_fusion.14
  177.6 1.3 copy.144
  180.8 1.3 constant_dynamic-slice_fusion.15
  182.1 2.1 constant_dynamic-slice_fusion.16
  184.2 2.1 constant_dynamic-slice_fusion.14
  187.3 1.3 copy.144
  190.6 1.3 constant_dynamic-slice_fusion.15
  191.9 2.1 constant_dynamic-slice_fusion.16
  193.9 2.1 constant_dynamic-slice_fusion.14
  197.0 1.3 copy.144
  200.3 1.3 constant_dynamic-slice_fusion.15
  201.6 2.1 constant_dynamic-slice_fusion.16
  203.7 2.1 constant_dynamic-slice_fusion.14
  206.8 1.3 copy.144
  210.0 1.3 constant_dynamic-slice_fusion.15
  211.3 2.1 constant_dynamic-slice_fusion.16
  213.4 2.1 constant_dynamic-slice_fusion.14
  216.5 1.3 copy.144
  219.7 1.3 constant_dynamic-slice_fusion.15
  221.0 2.1 constant_dynamic-slice_fusion.16
  223.1 2.1 constant_dynamic-slice_fusion.14
  226.2 1.3 copy.144
  229.1 4.1 all-to-all-start
  234.6 3.0 all-to-all-done
  237.6 3.3 all-to-all-start.1
  241.2 2.1 fusion.53
  243.2 2.1 all-to-all-done.1
  247.3 1.2 reshape.376
  248.5 115.7 %all_to_all.48 = bf16[64,4,2048]{2,1,0:T(4,128)(2,1)S(1)} all-to-all(bf16[64,4,2048]{2,1,0:T(4,128)(2,1)} %reshape.376), channel_id=1, replica_groups=mesh['sp'=64,'tp'=4] {'sp'}, dimensions={0} | all-to-all | bytes 2097152 | tf_op jit(solution)/shard_map/all_to_all | solution.py:214
  365.3 45.8 %all-gather.5.cloned.1.call-done = bf16[1024,2048]{1,0:T(8,128)(2,1)} async-done(((bf16[256,2048]{1,0:T(8,128)(2,1)}), bf16[1024,2048]{1,0:T(8,128)(2,1)}) %all-gather.5.cloned.1.call-update) | async-done | bytes 4194320 | tf_op jit(solution)/shard_map/all_gather | solution.py:215
  411.1 4.8 fusion.39
  415.9 9.1 %convolution_convert_fusion = bf16[1024,2048]{1,0:T(8,128)(2,1)} fusion(bf16[1024,2048]{1,0:T(8,128)(2,1)} %all-gather.5.cloned.1.call-done, bf16[1,256,2048]{2,1,0:T(8,128)(2,1)S(1)} %copy-done.31, bf16[1,2048,256]{2,1,0:T(8,128)(2,1)} %param.38, f32[1024,256]{1,0:T(8,128)} %fusion.39), kind=kOutput, calls=%fused_computation.63 | convolution fusion | flops 2151153664 | bytes 11534336 | tf_op jit(solution)/shard_map/dot_general | solution.py:220
  425.0 50.0 %reduce-scatter.2.cloned.1.call-done = bf16[256,2048]{1,0:T(8,128)(2,1)} async-done(((bf16[1024,2048]{1,0:T(8,128)(2,1)}), bf16[256,2048]{1,0:T(8,128)(2,1)}) %reduce-scatter.2.cloned.1.call-update) | async-done | bytes 1048592 | tf_op jit(solution)/shard_map/reduce_scatter | solution.py:219
  475.0 2.2 reshape.378
  477.2 10.9 %all-to-all-start.3 = ((bf16[64,4,2048]{2,1,0:T(4,128)(2,1)}), bf16[64,4,2048]{2,1,0:T(4,128)(2,1)}, u32[]{:S(2)}, u32[]{:S(2)}) async-start(bf16[64,4,2048]{2,1,0:T(4,128)(2,1)} %reshape.378), calls=%async_computation.4 | async-start | bytes 2097152 | tf_op jit(solution)/shard_map/all_to_all | solution.py:225
  488.7 27.6 %all-to-all-done.3 = bf16[64,4,2048]{2,1,0:T(4,128)(2,1)} async-done(((bf16[64,4,2048]{2,1,0:T(4,128)(2,1)}), bf16[64,4,2048]{2,1,0:T(4,128)(2,1)}, u32[]{:S(2)}, u32[]{:S(2)}) %all-to-all-start.3) | async-done | bytes 1048608 | tf_op jit(solution)/shard_map/all_to_all | solution.py:225
  516.2 1.3 reshape.379
  517.6 1.7 gather_fusion
  519.3 1.4 gather.7
  520.7 2.5 multiply_reduce_fusion
  (208 shorter events, 52.5 us)
Async XLA Ops:
  6.5 238.8 %copy-start = (bf16[512,2048]{1,0:T(8,128)(2,1)S(1)}, bf16[512,2048]{1,0:T(8,128)(2,1)}, u32[]{:S(2)}) copy-start(bf16[512,2048]{1,0:T(8,128)(2,1)} %param.33) | copy-start | bytes 6291460
  6.5 114.8 %all-gather.3.cloned.1.call-start = ((), (), s32[]{:S(2)}) async-start(), calls=%async_computation.5 | async-start | bytes 17039360 | tf_op jit(solution)/shard_map/all_gather | solution.py:15
  14.3 3.9 copy-start.25
  73.7 13.8 %copy-start.22 = (s32[64,2]{0,1:T(2,128)S(1)}, s32[64,2]{0,1:T(2,128)}, u32[]{:S(2)}) copy-start(s32[64,2]{0,1:T(2,128)} %param.35) | copy-start | bytes 1540
  73.7 15.0 %copy-start.9 = (bf16[256,128]{1,0:T(8,128)(2,1)S(1)}, bf16[256,128]{1,0:T(8,128)(2,1)}, u32[]{:S(2)}) copy-start(bf16[256,128]{1,0:T(8,128)(2,1)} %param.24) | copy-start | bytes 196612
  148.3 1.9 copy-start.11
  148.5 2.3 copy-start.20
  148.5 2.9 copy-start.1
  148.5 2.9 copy-start.17
  148.5 2.9 copy-start.30
  150.8 1.5 copy-start.8
  150.8 1.4 copy-start.21
  151.4 1.3 copy-start.14
  152.8 1.2 copy-start.15
  153.9 1.8 copy-start.10
  154.2 2.3 copy-start.18
  154.2 2.8 copy-start.2
  154.2 2.8 copy-start.16
  154.2 2.8 copy-start.29
  156.5 1.4 copy-start.7
  156.5 1.3 copy-start.19
  157.0 1.3 copy-start.12
  158.3 1.2 copy-start.13
  227.6 17.8 %copy-start.5 = (bf16[64,2048]{1,0:T(8,128)(2,1)S(1)}, bf16[64,2048]{1,0:T(8,128)(2,1)}, u32[]{:S(2)}) copy-start(bf16[64,2048]{1,0:T(8,128)(2,1)} %param.23) | copy-start | bytes 786436
  229.1 8.6 %all-to-all-start = ((bf16[4,64,128]{2,1,0:T(8,128)(2,1)}), bf16[4,64,128]{2,1,0:T(8,128)(2,1)S(1)}, u32[]{:S(2)}, u32[]{:S(2)}) async-start(bf16[4,64,128]{2,1,0:T(8,128)(2,1)} %bitcast.37), calls=%async_computation | async-start | bytes 131072 | tf_op jit(solution)/shard_map/all_to_all | solution.py:189
  237.6 7.7 %all-to-all-start.1 = ((bf16[4,64,128]{2,1,0:T(8,128)(2,1)}), bf16[4,64,128]{2,1,0:T(8,128)(2,1)S(1)}, u32[]{:S(2)}, u32[]{:S(2)}) async-start(bf16[4,64,128]{2,1,0:T(8,128)(2,1)} %bitcast.43), calls=%async_computation.1 | async-start | bytes 131072 | tf_op jit(solution)/shard_map/all_to_all | solution.py:190
  240.9 170.2 %all-gather.5.cloned.1.call-start = ((), (), s32[]{:S(2)}) async-start(), calls=%async_computation.6 | async-start | bytes 5242880 | tf_op jit(solution)/shard_map/all_gather | solution.py:215
  243.2 3.6 copy-start.6
  243.2 3.6 copy-start.24
  246.0 0.8 copy-start.3
  365.3 50.6 %copy-start.31 = (bf16[1,256,2048]{2,1,0:T(8,128)(2,1)S(1)}, bf16[1,256,2048]{2,1,0:T(8,128)(2,1)}, u32[]{:S(2)}) copy-start(bf16[1,256,2048]{2,1,0:T(8,128)(2,1)} %param.39) | copy-start | bytes 3145732
  365.3 109.7 %reduce-scatter.2.cloned.1.call-start = ((), (), s32[]{:S(2)}) async-start(), calls=%async_computation.7 | async-start | bytes 5242880 | tf_op jit(solution)/shard_map/reduce_scatter | solution.py:219
  425.0 63.2 %copy-start.23 = (s32[64,2]{0,1:T(2,128)S(1)}, s32[64,2]{0,1:T(2,128)}, u32[]{:S(2)}) copy-start(s32[64,2]{0,1:T(2,128)} %param.35) | copy-start | bytes 1540
  425.0 63.4 %copy-start.28 = (f32[64,2]{0,1:T(2,128)S(1)}, f32[64,2]{0,1:T(2,128)}, u32[]{:S(2)}) copy-start(f32[64,2]{0,1:T(2,128)} %param.36) | copy-start | bytes 1540
  425.0 63.5 %copy-start.27 = (pred[64,2]{0,1:T(4,128)(4,1)S(1)}, pred[64,2]{0,1:T(4,128)(4,1)}, u32[]{:S(2)}) copy-start(pred[64,2]{0,1:T(4,128)(4,1)} %get-tuple-element.875) | copy-start | bytes 388
  425.0 63.6 %copy-start.26 = (s32[128]{0:T(128)S(1)}, s32[128]{0:T(128)}, u32[]{:S(2)}) copy-start(s32[128]{0:T(128)} %copy-done.25) | copy-start | bytes 1540
  477.2 39.0 %all-to-all-start.3 = ((bf16[64,4,2048]{2,1,0:T(4,128)(2,1)}), bf16[64,4,2048]{2,1,0:T(4,128)(2,1)}, u32[]{:S(2)}, u32[]{:S(2)}) async-start(bf16[64,4,2048]{2,1,0:T(4,128)(2,1)} %reshape.378), calls=%async_computation.4 | async-start | bytes 2097152 | tf_op jit(solution)/shard_map/all_to_all | solution.py:225
  519.3 4.0 copy-start.4
Sparse Core Ops, SparseCore 0:
  11.3 110.0 all-gather.2
  365.4 45.6 all-gather.4
  425.1 49.8 reduce-scatter.1
where the time goes:
time: 533 us; the launch traced here: 531 us
  blocking collectives  164 us (31%)
  waiting for transfers between devices  161 us (30%)
  local copies, waits for them, and re-layouts  127 us (24%)
  matrix products  23.7 us (4%)
  starting transfers between devices  18.5 us (3%)
  other arithmetic  16.4 us (3%)
  between operations  13.5 us (3%)
  loops' own time  6.28 us (1%)
    all_to_all x1, blocking collectives, body(): lax.all_to_all(outgoing, 'sp', split_axis=0, concat_axis=0, tiled=True)  116 us
    dynamic_slice x32, local copies, waits for them, and re-layouts, take_block(): return lax.dynamic_slice_in_dim(source, inside, block_size, 0)  51.8 us
    reduce_scatter x1, waiting for transfers between devices, body(): lax.psum_scatter(jnp.dot(hidden, down_weight[0], preferred_element_type=j...  50 us
    all_gather x1, blocking collectives, sent_together(): whole, at, outs = (lax.all_gather(both, axis, axis=dim, tiled=True), 0, [])  48.7 us
    all_gather x1, waiting for transfers between devices, body(): lax.all_gather(arrived.reshape(-1, features), 'tp', axis=0, tiled=True)  45.8 us
    all_gather x1, waiting for transfers between devices, sent_together(): whole, at, outs = (lax.all_gather(both, axis, axis=dim, tiled=True), 0, [])  32 us
    all_to_all x1, waiting for transfers between devices, body(): lax.all_to_all(answers.reshape(expert_count, capacity, features), 'sp', s...  27.6 us
    slice x4, local copies, waits for them, and re-layouts, sent_together(): outs.append(lax.slice_in_dim(whole, at, at + a.shape[along], axis=along))  17.3 us
  transfers between devices with their start and end apart: 6, of which 6 were waited for; matrix products, arithmetic and copies ran while one was open for 6% of the time, Pallas kernels for 0%

commit v1 on v0

--- a/solution.py
+++ b/solution.py
@@ -212,7 +212,10 @@
     outgoing = jnp.dot(picker, normed, preferred_element_type=jnp.float32).astype(jnp.bfloat16)
     outgoing = outgoing.reshape(expert_count, capacity, features)
     arrived = lax.all_to_all(outgoing, "sp", split_axis=0, concat_axis=0, tiled=True)
-    pooled = lax.all_gather(arrived.reshape(-1, features), "tp", axis=0, tiled=True)
+    x = arrived.reshape(-1, features)
+    size = lax.axis_size("tp")
+    repeats = [size if d == 0 else 1 for d in range(x.ndim)]
+    pooled = lax.all_to_all(jnp.tile(x, repeats), "tp", split_axis=0, concat_axis=0, tiled=True)
     gate_value = jnp.dot(pooled, gate_weight[0], preferred_element_type=jnp.float32)
     up_value = jnp.dot(pooled, up_weight[0], preferred_element_type=jnp.float32)
     hidden = (jax.nn.silu(gate_value) * up_value).astype(jnp.bfloat16)

time: 533 us -> 535 us (level)
  blocking collectives: 164 us -> 215 us
  waiting for transfers between devices: 161 us -> 110 us
    all_to_all x0 -> x1, blocking collectives: none -> 50.4 us  [body(): lax.all_to_all(jnp.tile(x, repeats), 'tp', split_axis=0, concat_axis=0, t...]
    all_gather x1 -> x0, waiting for transfers between devices: 45.8 us -> none  [body(): lax.all_gather(arrived.reshape(-1, features), 'tp', axis=0, tiled=True)]
  transfers between devices with their start and end apart: 6 -> 5, of which waited for: 6 -> 5; matrix products, arithmetic and copies ran while one was open for 6% -> 6% of each run, Pallas kernels for 0% -> 0%
where the time goes in v1:
time: 535 us; the launch traced here: 533 us
  blocking collectives  215 us (40%)
  local copies, waits for them, and re-layouts  131 us (24%)
  waiting for transfers between devices  110 us (21%)
  matrix products  21.2 us (4%)
  starting transfers between devices  18.4 us (3%)
  other arithmetic  16.9 us (3%)
  between operations  13.8 us (3%)
  loops' own time  6.28 us (1%)
    all_to_all x1, blocking collectives, body(): lax.all_to_all(outgoing, 'sp', split_axis=0, concat_axis=0, tiled=True)  116 us
    dynamic_slice x32, local copies, waits for them, and re-layouts, take_block(): return lax.dynamic_slice_in_dim(source, inside, block_size, 0)  52 us
    all_to_all x1, blocking collectives, body(): lax.all_to_all(jnp.tile(x, repeats), 'tp', split_axis=0, concat_axis=0, t...  50.4 us
    all_gather x1, blocking collectives, sent_together(): whole, at, outs = (lax.all_gather(both, axis, axis=dim, tiled=True), 0, [])  48.7 us
    reduce_scatter x1, waiting for transfers between devices, body(): lax.psum_scatter(jnp.dot(hidden, down_weight[0], preferred_element_type=j...  45.6 us
    all_gather x1, waiting for transfers between devices, sent_together(): whole, at, outs = (lax.all_gather(both, axis, axis=dim, tiled=True), 0, [])  31.6 us
    all_to_all x1, waiting for transfers between devices, body(): lax.all_to_all(answers.reshape(expert_count, capacity, features), 'sp', s...  27.6 us
    slice x4, local copies, waits for them, and re-layouts, sent_together(): outs.append(lax.slice_in_dim(whole, at, at + a.shape[along], axis=along))  17.3 us
  transfers between devices with their start and end apart: 5, of which 5 were waited for; matrix products, arithmetic and copies ran while one was open for 6% of the time, Pallas kernels for 0%

profile of v1, /device:TPU:1, one launch (start us, length us, event | category | flops | bytes accessed | tf_op | source)
XLA Modules:
  0.0 532.9 jit_solution(12834658208189892232)
XLA Ops:
  18.3 48.7 %all_gather.7 = f32[16384,3]{0,1:T(4,128)S(1)} all-gather(f32[256,3]{0,1:T(4,128)S(1)} %pad_maximum_fusion.3), channel_id=1, replica_groups=mesh['sp'=64,'tp'=4] {'sp'}, dimensions={0}, use_global_device_ids=true | all-gather | bytes 199680 | tf_op jit(solution)/shard_map/all_gather | solution.py:15
  67.1 5.0 copy.106
  72.0 1.5 reduce-window_subtract_fusion
  74.0 9.2 %reshape.391 = f32[64,256,1]{2,1,0:T(8,128)} reshape(f32[16384]{0:T(1024)S(1)} %slice_reduce_fusion) | data formatting | bytes 131072 | tf_op jit(solution)/shard_map/reshape | solution.py:24
  83.2 2.0 fusion.75
  89.9 31.6 %all-gather.2.cloned.1.call-done = bf16[16384,512]{0,1:T(8,128)(2,1)} async-done(((bf16[256,512]{0,1:T(8,128)(2,1)}), bf16[16384,512]{0,1:T(8,128)(2,1)}) %all-gather.2.cloned.1.call-update) | async-done | bytes 16777232 | tf_op jit(solution)/shard_map/all_gather | solution.py:15
  121.5 12.1 %fusion.72 = (bf16[16384,128]{0,1:T(8,128)(2,1)}, bf16[16384,128]{0,1:T(8,128)(2,1)}, bf16[16384,128]{0,1:T(8,128)(2,1)}, bf16[16384,128]{0,1:T(8,128)(2,1)}) fusion(bf16[16384,512]{0,1:T(8,128)(2,1)} %all-gather.2.cloned.1.call-done), kind=kLoop, calls=%fused_computation.146 | loop fusion | bytes 33554432 | tf_op jit(solution)/shard_map/slice | solution.py:17
  138.7 89.9 %while.35 = (s32[]{:T(128)}, f32[1,128]{1,0:T(1,128)}, f32[1,128]{1,0:T(1,128)}, f32[1,128,128]{2,1,0:T(8,128)S(1)}, f32[2,128]{1,0:T(2,128)}, /*index=5*/f32[2,...) while((s32[]{:T(128)}, f32[1,128]{1,0:T(1,128)}, ...), condition=%wide.region_19.20_spmd, body=%wide.region_6.19_spmd.sunk | while | flops 552212480 | bytes 35769752 | solution.py:180
  138.7 1.3 dynamic_slice.78
  140.6 1.3 constant_dynamic-slice_fusion.15
  141.9 2.1 constant_dynamic-slice_fusion.16
  144.0 2.1 constant_dynamic-slice_fusion.14
  147.1 1.3 copy.144
  148.4 5.7 %conditional.4 = ((f32[1,128]{1,0:T(1,128)}, f32[1,128]{1,0:T(1,128)}, f32[1,128,128]{2,1,0:T(8,128)S(1)}, f32[2,128]{1,0:T(2,128)}, f32[2,128]{1,0:T(2,128)}, /*index=5*/f32[2,128,64]{1,2,0:T(8,128)S(1)})) conditional(s32[]{:T(128)} %convert_element_type.151, (f32[1,128]{1,0:T(1,128)}, f32[1,128]{1,0:T(1,128)}, f32[1,128,128]{2,1,0:T(8,128)S(1)}, ...), branch_computations={%region_7.7_spmd, %region_8.12_spmd} | conditional | flops 276106240 | bytes 14714172 | solution.py:175
  148.8 1.5 fusion.68
  154.1 5.7 %conditional.5 = ((f32[1,128]{1,0:T(1,128)}, f32[1,128]{1,0:T(1,128)}, f32[1,128,128]{2,1,0:T(8,128)S(1)}, f32[2,128]{1,0:T(2,128)}, f32[2,128]{1,0:T(2,128)}, /*index=5*/f32[2,128,64]{1,2,0:T(8,128)S(1)})) conditional(s32[]{:T(128)} %convert_element_type.152, (f32[1,128]{1,0:T(1,128)}, f32[1,128]{1,0:T(1,128)}, f32[1,128,128]{2,1,0:T(8,128)S(1)}, ...), branch_computations={%region_13.13_spmd, %region_14.18_spmd} | conditional | flops 276106240 | bytes 14714172 | solution.py:175
  154.4 1.5 fusion.70
  161.7 1.3 constant_dynamic-slice_fusion.15
  163.0 2.1 constant_dynamic-slice_fusion.16
  165.1 2.1 constant_dynamic-slice_fusion.14
  168.2 1.3 copy.144
  171.5 1.3 constant_dynamic-slice_fusion.15
  172.8 2.1 constant_dynamic-slice_fusion.16
  174.9 2.1 constant_dynamic-slice_fusion.14
  178.0 1.3 copy.144
  181.4 1.3 constant_dynamic-slice_fusion.15
  182.7 2.1 constant_dynamic-slice_fusion.16
  184.7 2.1 constant_dynamic-slice_fusion.14
  187.9 1.3 copy.144
  191.2 1.3 constant_dynamic-slice_fusion.15
  192.5 2.1 constant_dynamic-slice_fusion.16
  194.6 2.1 constant_dynamic-slice_fusion.14
  197.7 1.3 copy.144
  201.0 1.3 constant_dynamic-slice_fusion.15
  202.3 2.1 constant_dynamic-slice_fusion.16
  204.4 2.1 constant_dynamic-slice_fusion.14
  207.5 1.3 copy.144
  210.8 1.3 constant_dynamic-slice_fusion.15
  212.1 2.1 constant_dynamic-slice_fusion.16
  214.2 2.1 constant_dynamic-slice_fusion.14
  217.3 1.3 copy.144
  220.7 1.3 constant_dynamic-slice_fusion.15
  222.0 2.1 constant_dynamic-slice_fusion.16
  224.0 2.1 constant_dynamic-slice_fusion.14
  227.2 1.3 copy.144
  230.0 4.0 all-to-all-start
  235.4 3.0 all-to-all-done
  238.5 3.3 all-to-all-start.1
  242.0 2.1 fusion.53
  244.1 2.1 all-to-all-done.1
  249.4 116.2 %all_to_all.57 = bf16[64,4,2048]{2,1,0:T(4,128)(2,1)} all-to-all(bf16[64,4,2048]{2,1,0:T(4,128)(2,1)} %reshape.380), channel_id=1, replica_groups=mesh['sp'=64,'tp'=4] {'sp'}, dimensions={0} | all-to-all | bytes 2097152 | tf_op jit(solution)/shard_map/all_to_all | solution.py:214
  365.6 1.3 tile.8
  367.5 50.4 %all_to_all.58 = bf16[4,256,2048]{2,1,0:T(8,128)(2,1)S(1)} all-to-all(bf16[4,256,2048]{2,1,0:T(8,128)(2,1)S(1)} %tile.9), channel_id=1, replica_groups=mesh['sp'=64,'tp'=4] {'tp'}, dimensions={0} | all-to-all | bytes 8388608 | tf_op jit(solution)/shard_map/all_to_all | solution.py:218
  417.9 2.0 copy-done.5
  419.9 2.3 fusion.39
  422.2 9.1 %convolution_convert_fusion = bf16[1024,2048]{1,0:T(8,128)(2,1)} fusion(bf16[1024,2048]{1,0:T(8,128)(2,1)} %bitcast.142, bf16[1,256,2048]{2,1,0:T(8,128)(2,1)S(1)} %copy-done.33, bf16[1,2048,256]{2,1,0:T(8,128)(2,1)} %param.38, f32[1024,256]{1,0:T(8,128)} %fusion.39), kind=kOutput, calls=%fused_computation.63 | convolution fusion | flops 2151153664 | bytes 11534336 | tf_op jit(solution)/shard_map/dot_general | solution.py:223
  431.3 45.6 %reduce-scatter.2.cloned.1.call-done = bf16[256,2048]{1,0:T(8,128)(2,1)} async-done(((bf16[1024,2048]{1,0:T(8,128)(2,1)}), bf16[256,2048]{1,0:T(8,128)(2,1)}) %reduce-scatter.2.cloned.1.call-update) | async-done | bytes 1048592 | tf_op jit(solution)/shard_map/reduce_scatter | solution.py:222
  477.0 2.3 reshape.381
  479.2 10.9 %all-to-all-start.4 = ((bf16[64,4,2048]{2,1,0:T(4,128)(2,1)}), bf16[64,4,2048]{2,1,0:T(4,128)(2,1)}, u32[]{:S(2)}, u32[]{:S(2)}) async-start(bf16[64,4,2048]{2,1,0:T(4,128)(2,1)} %reshape.381), calls=%async_computation.5 | async-start | bytes 2097152 | tf_op jit(solution)/shard_map/all_to_all | solution.py:228
  490.7 27.6 %all-to-all-done.4 = bf16[64,4,2048]{2,1,0:T(4,128)(2,1)} async-done(((bf16[64,4,2048]{2,1,0:T(4,128)(2,1)}), bf16[64,4,2048]{2,1,0:T(4,128)(2,1)}, u32[]{:S(2)}, u32[]{:S(2)}) %all-to-all-start.4) | async-done | bytes 1048608 | tf_op jit(solution)/shard_map/all_to_all | solution.py:228
  518.2 1.3 reshape.382
  519.6 1.7 gather_fusion
  521.3 1.4 gather.7
  522.7 2.5 multiply_reduce_fusion
  (211 shorter events, 55.1 us)
Async XLA Ops:
  6.5 239.7 %copy-start = (bf16[512,2048]{1,0:T(8,128)(2,1)S(1)}, bf16[512,2048]{1,0:T(8,128)(2,1)}, u32[]{:S(2)}) copy-start(bf16[512,2048]{1,0:T(8,128)(2,1)} %param.33) | copy-start | bytes 6291460
  6.5 114.9 %all-gather.2.cloned.1.call-start = ((), (), s32[]{:S(2)}) async-start(), calls=%async_computation.6 | async-start | bytes 17039360 | tf_op jit(solution)/shard_map/all_gather | solution.py:15
  14.3 3.9 copy-start.26
  74.0 14.0 %copy-start.23 = (s32[64,2]{0,1:T(2,128)S(1)}, s32[64,2]{0,1:T(2,128)}, u32[]{:S(2)}) copy-start(s32[64,2]{0,1:T(2,128)} %param.35) | copy-start | bytes 1540
  74.0 15.2 %copy-start.10 = (bf16[256,128]{1,0:T(8,128)(2,1)S(1)}, bf16[256,128]{1,0:T(8,128)(2,1)}, u32[]{:S(2)}) copy-start(bf16[256,128]{1,0:T(8,128)(2,1)} %param.24) | copy-start | bytes 196612
  148.5 1.9 copy-start.12
  148.7 2.3 copy-start.21
  148.7 2.9 copy-start.1
  148.7 2.9 copy-start.18
  148.8 2.8 copy-start.31
  151.0 1.4 copy-start.9
  151.0 1.4 copy-start.22
  151.6 1.3 copy-start.15
  152.9 1.2 copy-start.16
  154.1 1.8 copy-start.11
  154.4 2.3 copy-start.19
  154.4 2.9 copy-start.2
  154.4 2.9 copy-start.17
  154.4 2.9 copy-start.30
  156.7 1.5 copy-start.8
  156.7 1.4 copy-start.20
  157.3 1.3 copy-start.13
  158.6 1.2 copy-start.14
  228.5 17.7 %copy-start.6 = (bf16[64,2048]{1,0:T(8,128)(2,1)S(1)}, bf16[64,2048]{1,0:T(8,128)(2,1)}, u32[]{:S(2)}) copy-start(bf16[64,2048]{1,0:T(8,128)(2,1)} %param.23) | copy-start | bytes 786436
  230.0 8.5 %all-to-all-start = ((bf16[4,64,128]{2,1,0:T(8,128)(2,1)}), bf16[4,64,128]{2,1,0:T(8,128)(2,1)S(1)}, u32[]{:S(2)}, u32[]{:S(2)}) async-start(bf16[4,64,128]{2,1,0:T(8,128)(2,1)} %bitcast.37), calls=%async_computation | async-start | bytes 131072 | tf_op jit(solution)/shard_map/all_to_all | solution.py:189
  238.5 7.7 %all-to-all-start.1 = ((bf16[4,64,128]{2,1,0:T(8,128)(2,1)}), bf16[4,64,128]{2,1,0:T(8,128)(2,1)S(1)}, u32[]{:S(2)}, u32[]{:S(2)}) async-start(bf16[4,64,128]{2,1,0:T(8,128)(2,1)} %bitcast.43), calls=%async_computation.1 | async-start | bytes 131072 | tf_op jit(solution)/shard_map/all_to_all | solution.py:190
  241.8 235.2 %reduce-scatter.2.cloned.1.call-start = ((), (), s32[]{:S(2)}) async-start(), calls=%async_computation.7 | async-start | bytes 5242880 | tf_op jit(solution)/shard_map/reduce_scatter | solution.py:222
  244.1 3.6 copy-start.7
  244.1 3.6 copy-start.25
  246.8 0.8 copy-start.3
  367.4 52.4 %copy-start.32 = (bf16[1,2048,256]{2,1,0:T(8,128)(2,1)S(1)}, bf16[1,2048,256]{2,1,0:T(8,128)(2,1)}, u32[]{:S(2)}) copy-start(bf16[1,2048,256]{2,1,0:T(8,128)(2,1)} %param.37) | copy-start | bytes 3145732
  417.9 2.0 copy-start.5
  419.9 2.3 copy-start.33
  431.3 58.9 %copy-start.24 = (s32[64,2]{0,1:T(2,128)S(1)}, s32[64,2]{0,1:T(2,128)}, u32[]{:S(2)}) copy-start(s32[64,2]{0,1:T(2,128)} %param.35) | copy-start | bytes 1540
  431.3 59.1 %copy-start.29 = (f32[64,2]{0,1:T(2,128)S(1)}, f32[64,2]{0,1:T(2,128)}, u32[]{:S(2)}) copy-start(f32[64,2]{0,1:T(2,128)} %param.36) | copy-start | bytes 1540
  431.3 59.2 %copy-start.28 = (pred[64,2]{0,1:T(4,128)(4,1)S(1)}, pred[64,2]{0,1:T(4,128)(4,1)}, u32[]{:S(2)}) copy-start(pred[64,2]{0,1:T(4,128)(4,1)} %get-tuple-element.875) | copy-start | bytes 388
  431.3 59.3 %copy-start.27 = (s32[128]{0:T(128)S(1)}, s32[128]{0:T(128)}, u32[]{:S(2)}) copy-start(s32[128]{0:T(128)} %copy-done.26) | copy-start | bytes 1540
  479.2 39.0 %all-to-all-start.4 = ((bf16[64,4,2048]{2,1,0:T(4,128)(2,1)}), bf16[64,4,2048]{2,1,0:T(4,128)(2,1)}, u32[]{:S(2)}, u32[]{:S(2)}) async-start(bf16[64,4,2048]{2,1,0:T(4,128)(2,1)} %reshape.381), calls=%async_computation.5 | async-start | bytes 2097152 | tf_op jit(solution)/shard_map/all_to_all | solution.py:228
  521.3 4.0 copy-start.4
Sparse Core Ops, SparseCore 0:
  11.3 110.0 all-gather.1
  431.4 45.5 reduce-scatter.1
